TPU v7x, 32 devices: a whole 2x2x4 slice. The times are simulated.
32 devices in a mesh: sp: 8 (over z, core), tp: 4 (over y, x).
Axes of the slice: x: 2, y: 2, z: 4, core: 2. Of those that a mesh axis runs over, the one named last changes fastest.
Arguments:
- stream: bfloat16 [3072, 2048], P('sp'), may hold values from -6 to 6
- inner_act: bfloat16 [3072, 4096], P('sp', 'tp'), may hold values from -6 to 6
- gate_act: bfloat16 [3072, 4096], P('sp', 'tp'), may hold values from -6 to 6
- state_write: bfloat16 [3072, 16, 128], P('sp', 'tp'), may hold values from -6 to 6
- state_read: bfloat16 [3072, 16, 128], P('sp', 'tp'), may hold values from -6 to 6
- step_raw: bfloat16 [3072, 64], P('sp', 'tp'), may hold values from -4.6 to 4.1
- conv_inner: bfloat16 [4, 4096], P(None, 'tp'), may hold values from -3 to 3
- conv_write: bfloat16 [4, 16, 128], P(None, 'tp'), may hold values from -3 to 3
- conv_read: bfloat16 [4, 16, 128], P(None, 'tp'), may hold values from -3 to 3
- step_bias: float32 [64], P('tp'), may hold values from -0.5 to 0.5
- decay_log: float32 [64], P('tp'), may hold values from -13 to -2.52, as said below
- inner_gain: float32 [4096], P('tp'), may hold values from 0.1 to 1.9
- out_weight: bfloat16 [4096, 2048], P('tp'), may hold values from -0.09375 to 0.09375
- ffn_gain: float32 [2048], replicated, may hold values from 0.1 to 1.9
- expert_ids: int32 [3072, 2], P('sp'), may hold values from 0 to 31, all different within a row; in each aligned block of 384 rows (0 to 383, 384 to 767, ...) at most 48 rows name the same one
- expert_weights: float32 [3072, 2], P('sp'), may hold values from 0.1 to 1
- expert_gate: bfloat16 [32, 2048, 1024], P('sp', None, 'tp'), may hold values from -0.125 to 0.125
- expert_up: bfloat16 [32, 2048, 1024], P('sp', None, 'tp'), may hold values from -0.125 to 0.125
- expert_down: bfloat16 [32, 1024, 2048], P('sp', None, 'tp'), may hold values from -0.1875 to 0.1875
Outputs:
- layer_out: bfloat16 [3072, 2048], P('sp', 'tp')
Inputs may be any that keep to these rules, and one draw needn't show every extreme that they name: The logarithm of a per-position decay rate: exp(decay_log) lies between 0.1 / 3072 and 0.08. `expert_ids`: each row names 2 different experts. Among the rows of one index of sp (384 tokens) no expert is named more than 48 times, a bound that some block reaches there.
All inputs are finite; a program needn't handle non-finite values.
Results may differ from a plain program's by a relative error of at most 0.014.
Values may be sent and summed in bfloat16 or wider, within the bound.
A program may use at most 64 MiB of HBM per device.

v0:
```python
import functools

import jax
import jax.numpy as jnp
from jax import lax
from jax.experimental import pallas as pl
from jax.experimental.pallas import tpu as pltpu
from jax.sharding import PartitionSpec as P

TOPK = 2
CAP = 48
EPS = 1e-06
HIGH = lax.Precision.HIGHEST
MESH = pl.DeviceIdType.MESH
HALO = 8
VMEM = pl.BlockSpec(memory_space=pltpu.VMEM)
ANY = pl.BlockSpec(memory_space=pl.ANY)
F32 = jnp.float32
BF16 = jnp.bfloat16


def silu(x):
    return x / (1.0 + jnp.exp(-x))


def nt_dot(a, b):
    return lax.dot_general(a, b, (((1,), (1,)), ((), ())), preferred_element_type=F32)


def tn_dot(a, b):
    return lax.dot_general(a, b, (((0,), (0,)), ((), ())), preferred_element_type=F32)


def conv_kernel(
    per_group, x_ref, w_ref, r_ref, hx_ref, hw_ref, hr_ref, kx_ref, kw_ref, kr_ref, end_ref,
    xs_ref, bw_ref, cr_ref, state_ref, pad_ref,
):
    length = x_ref.shape[0]

    def conv(src_ref, halo_ref, tap_ref):
        width = src_ref.shape[1]
        pad_ref[0:HALO, 0:width] = halo_ref[...].astype(F32)
        pad_ref[HALO : HALO + length, 0:width] = src_ref[...].astype(F32)
        taps = tap_ref[...].astype(F32)
        count = taps.shape[0]
        total = jnp.zeros((length, width), F32)
        for k in range(count):
            begin = HALO + k - count + 1
            total = total + taps[k : k + 1, :] * pad_ref[begin : begin + length, 0:width]
        return silu(total)

    xs = conv(x_ref, hx_ref, kx_ref)
    bw = conv(w_ref, hw_ref, kw_ref).astype(BF16)
    cr_ref[...] = conv(r_ref, hr_ref, kr_ref).astype(BF16)
    xs_ref[...] = xs.astype(BF16)
    bw_ref[...] = bw
    head_dim = xs.shape[1] // per_group
    scaled = [
        xs[:, h * head_dim : (h + 1) * head_dim] * end_ref[0, :, h : h + 1] for h in range(per_group)
    ]
    weighted = jnp.concatenate(scaled, axis=1).astype(BF16)
    state_ref[...] = tn_dot(weighted, bw).astype(BF16)


def inside_kernel(per_group, xs_ref, bw_ref, cr_ref, cum_ref, cumt_ref, stept_ref, out_ref):
    length = xs_ref.shape[0]
    head_dim = xs_ref.shape[1] // per_group
    scores = nt_dot(cr_ref[...], bw_ref[...])
    rows = lax.broadcasted_iota(jnp.int32, (length, length), 0)
    columns = lax.broadcasted_iota(jnp.int32, (length, length), 1)
    causal = rows >= columns
    pieces = []
    for h in range(per_group):
        spread = cum_ref[0, :, h : h + 1] - cumt_ref[0, h : h + 1, :]
        within = jnp.exp(jnp.where(causal, spread, -1e30))
        mixing = (scores * within * stept_ref[0, h : h + 1, :]).astype(BF16)
        pieces.append(
            jnp.dot(
                mixing, xs_ref[:, h * head_dim : (h + 1) * head_dim], preferred_element_type=F32
            )
        )
    out_ref[...] = jnp.concatenate(pieces, axis=1)


def outside_kernel(
    per_group, in_ref, cr_ref, state_ref, cum_ref, gate_ref, gain_ref, out_ref
):
    head_dim = in_ref.shape[1] // per_group
    outside = nt_dot(cr_ref[...], state_ref[...])
    gates = silu(gate_ref[...].astype(F32))
    pieces = []
    for h in range(per_group):
        cut = slice(h * head_dim, (h + 1) * head_dim)
        part = in_ref[:, cut] + outside[:, cut] * jnp.exp(cum_ref[0, :, h : h + 1])
        part = part * gates[:, cut]
        scale = lax.rsqrt(jnp.mean(part * part, axis=1, keepdims=True) + EPS)
        pieces.append(part * scale)
    out_ref[...] = (jnp.concatenate(pieces, axis=1) * gain_ref[...]).astype(BF16)


def experts_kernel(
    n_sp, n_tp, slots_ref, gate_hbm, up_hbm, down_hbm, back_ref,
    gate_ref, up_ref, down_ref, rows_ref, hid_ref, done_ref,
    w_sem, own_sem, s_send, s_recv, x_send, x_recv, y_send, y_recv, dx_send, dx_recv, dy_send, dy_recv,
    hx_send, hx_recv, hy_send, hy_recv, hdx_send, hdx_recv, hdy_send, hdy_recv, r_send, r_recv,
):
    me = lax.axis_index("sp")
    tp = lax.axis_index("tp")
    plane, core = me // 2, me % 2
    planes = n_sp // 2
    xp = tp + 1 - 2 * (tp % 2)
    yp = (tp + 2) % 4
    experts = gate_ref.shape[0]
    half = experts // 2
    cap = rows_ref.shape[3]
    share = rows_ref.shape[4]
    width = hid_ref.shape[4]

    barrier = pltpu.get_barrier_semaphore()
    for step in range(1, n_sp):
        pl.semaphore_signal(
            barrier, inc=1, device_id=((me + step) % n_sp, tp), device_id_type=MESH
        )
    for peer in (xp, yp):
        pl.semaphore_signal(barrier, inc=1, device_id=(me, peer), device_id_type=MESH)
    pl.semaphore_wait(barrier, n_sp + 1)

    sends = []

    def remote(src, dst, send, recv, device):
        return pltpu.make_async_remote_copy(
            src_ref=src, dst_ref=dst, send_sem=send, recv_sem=recv,
            device_id=device, device_id_type=MESH,
        )

    def start(copy):
        copy.start()
        sends.append(copy)

    own = pltpu.make_async_copy(slots_ref.at[me], rows_ref.at[tp, me], own_sem.at[0])
    own.start()
    for j in range(planes):
        for c in range(2):
            if j == 0 and c == 1:
                continue
            to_core = (core + 1) % 2 if j == 0 else c
            target = ((plane - j + planes) % planes) * 2 + to_core
            start(
                remote(
                    slots_ref.at[target], rows_ref.at[tp, me], s_send.at[j * 2 + c],
                    s_recv.at[j * 2 + core], (target, tp),
                )
            )
    loads = [
        pltpu.make_async_copy(a, b, w_sem.at[i])
        for i, (a, b) in enumerate(
            ((gate_hbm, gate_ref), (up_hbm, up_ref), (down_hbm, down_ref))
        )
    ]
    for load in loads:
        load.start()

    def source(j, c):
        return ((plane + j) % planes) * 2 + c

    def exchange(buf, j, c, sems):
        s = source(j, c)
        k = j * 2 + c
        piece = buf.at[tp, s]
        start(remote(piece, piece, sems[0].at[k], sems[1].at[k], (me, xp)))
        start(remote(piece, piece, sems[2].at[k], sems[3].at[k], (me, yp)))

    def relay(buf, j, c, near, far):
        s = source(j, c)
        k = j * 2 + c
        piece = buf.at[xp, s]
        remote(piece, piece, near[0].at[k], near[1].at[k], (me, xp)).wait_recv()
        part = buf.at[xp, s, pl.ds(0, half)]
        start(remote(part, part, far[2].at[k], far[3].at[k], (me, yp)))
        piece = buf.at[yp, s]
        remote(piece, piece, near[2].at[k], near[3].at[k], (me, yp)).wait_recv()
        part = buf.at[yp, s, pl.ds(half, experts - half)]
        start(remote(part, part, far[0].at[k], far[1].at[k], (me, xp)))

    def arrive(buf, j, c, far):
        s = source(j, c)
        k = j * 2 + c
        dp = (xp + 2) % 4
        part = buf.at[dp, s, pl.ds(0, half)]
        remote(part, part, far[2].at[k], far[3].at[k], (me, yp)).wait_recv()
        part = buf.at[dp, s, pl.ds(half, experts - half)]
        remote(part, part, far[0].at[k], far[1].at[k], (me, xp)).wait_recv()

    row_near = (x_send, x_recv, y_send, y_recv)
    row_far = (dx_send, dx_recv, dy_send, dy_recv)
    hid_near = (hx_send, hx_recv, hy_send, hy_recv)
    hid_far = (hdx_send, hdx_recv, hdy_send, hdy_recv)

    def stage_a(j):
        if j == 0:
            own.wait()
            other = (core + 1) % 2
            remote(
                rows_ref.at[tp, source(0, other)], rows_ref.at[tp, source(0, other)],
                s_send.at[0], s_recv.at[other], (source(0, other), tp),
            ).wait_recv()
        for c in range(2):
            if j > 0:
                piece = rows_ref.at[tp, source(j, c)]
                remote(
                    piece, piece, s_send.at[0], s_recv.at[j * 2 + c], (source(j, c), tp)
                ).wait_recv()
            exchange(rows_ref, j, c, row_near)

    def stage_b(j):
        for c in range(2):
            relay(rows_ref, j, c, row_near, row_far)

    def stage_c(j):
        if j == 0:
            loads[0].wait()
            loads[1].wait()
        for c in range(2):
            arrive(rows_ref, j, c, row_far)
        first = source(j, 0)

        def one(e, carry):
            gate = jnp.zeros((2 * cap, width), F32)
            up = jnp.zeros((2 * cap, width), F32)
            for q in range(n_tp):
                x = rows_ref[q, pl.ds(first, 2), e].reshape(2 * cap, share)
                cut = slice(q * share, (q + 1) * share)
                gate = gate + jnp.dot(x, gate_ref[e, cut, :], preferred_element_type=F32)
                up = up + jnp.dot(x, up_ref[e, cut, :], preferred_element_type=F32)
            hidden = (silu(gate) * up).astype(BF16)
            hid_ref[tp, pl.ds(first, 2), e] = hidden.reshape(2, cap, width)
            return carry

        lax.fori_loop(0, experts, one, 0)
        for c in range(2):
            exchange(hid_ref, j, c, hid_near)

    def stage_d(j):
        for c in range(2):
            relay(hid_ref, j, c, hid_near, hid_far)

    keep = []

    def stage_e(j):
        if j == 0:
            loads[2].wait()
        for c in range(2):
            arrive(hid_ref, j, c, hid_far)
        first = source(j, 0)

        def one(e, carry):
            total = jnp.zeros((2 * cap, share), F32)
            for q in range(n_tp):
                x = hid_ref[q, pl.ds(first, 2), e].reshape(2 * cap, width)
                cut = slice(q * width, (q + 1) * width)
                total = total + jnp.dot(x, down_ref[e, cut, :], preferred_element_type=F32)
            done_ref[pl.ds(first, 2), e] = total.astype(BF16).reshape(2, cap, share)
            return carry

        lax.fori_loop(0, experts, one, 0)
        if j == 0:
            copy = pltpu.make_async_copy(done_ref.at[me], back_ref.at[me], own_sem.at[1])
            copy.start()
            keep.append(copy)
        for c in range(2):
            if j == 0 and c == 1:
                continue
            target = source(0, (core + 1) % 2) if j == 0 else source(j, c)
            start(
                remote(
                    done_ref.at[target], back_ref.at[me], r_send.at[j * 2 + c],
                    r_recv.at[j * 2 + core], (target, tp),
                )
            )

    stages = (stage_a, stage_b, stage_c, stage_d, stage_e)
    lag = (0, 1, 2, 3, 4)
    for turn in range(planes + lag[-1]):
        for stage, late in zip(stages, lag):
            if 0 <= turn - late < planes:
                stage(turn - late)

    keep[0].wait()
    for j in range(planes):
        for c in range(2):
            if j == 0:
                if c == 1:
                    continue
                other = (core + 1) % 2
                origin, k = source(0, other), other
            else:
                origin, k = ((plane - j + planes) % planes) * 2 + c, j * 2 + c
            piece = back_ref.at[origin]
            remote(piece, piece, r_send.at[0], r_recv.at[k], (origin, tp)).wait_recv()
    for copy in sends:
        copy.wait_send()


def run_experts_plain(slots, expert_gate, expert_up, expert_down):
    experts, _, width = expert_gate.shape
    arrived = lax.all_to_all(slots, "sp", split_axis=0, concat_axis=0, tiled=True)
    rows = lax.all_gather(arrived, "tp", axis=3, tiled=True)
    gate = jnp.einsum("secd,edf->secf", rows, expert_gate, preferred_element_type=F32)
    up = jnp.einsum("secd,edf->secf", rows, expert_up, preferred_element_type=F32)
    hidden = lax.all_gather((jax.nn.silu(gate) * up).astype(BF16), "tp", axis=3, tiled=True)
    done = jnp.einsum("secf,efd->secd", hidden, expert_down, preferred_element_type=F32)
    return lax.all_to_all(done.astype(BF16), "sp", split_axis=0, concat_axis=0, tiled=True)


def run_experts(slots, expert_gate, expert_up, expert_down):
    n_sp, n_tp = lax.axis_size("sp"), lax.axis_size("tp")
    experts, full, width = expert_gate.shape
    share = expert_down.shape[2]
    if n_tp != 4 or n_sp % 2 or experts < 2:
        return run_experts_plain(slots, expert_gate, expert_up, expert_down)
    dma = lambda count: pltpu.SemaphoreType.DMA((count,))
    return pl.pallas_call(
        functools.partial(experts_kernel, n_sp, n_tp),
        out_shape=jax.ShapeDtypeStruct((n_sp, experts, CAP, share), BF16),
        in_specs=[VMEM, ANY, ANY, ANY],
        out_specs=VMEM,
        scratch_shapes=[
            pltpu.VMEM(expert_gate.shape, BF16),
            pltpu.VMEM(expert_up.shape, BF16),
            pltpu.VMEM(expert_down.shape, BF16),
            pltpu.VMEM((n_tp, n_sp, experts, CAP, share), BF16),
            pltpu.VMEM((n_tp, n_sp, experts, CAP, width), BF16),
            pltpu.VMEM((n_sp, experts, CAP, share), BF16),
            dma(3),
            dma(2),
        ]
        + [dma(n_sp) for _ in range(20)],
        compiler_params=pltpu.CompilerParams(
            collective_id=0, has_side_effects=True, vmem_limit_bytes=60 * 2**20
        ),
        cost_estimate=pl.CostEstimate(
            flops=10**10, bytes_accessed=2 * 10**7, transcendentals=10**6
        ),
    )(slots, expert_gate, expert_up, expert_down)


def per_device(
    stream, inner_act, gate_act, state_write, state_read, step_raw, conv_inner, conv_write, conv_read,
    step_bias, decay_log, inner_gain, out_weight, ffn_gain, expert_ids, expert_weights,
    expert_gate, expert_up, expert_down,
):
    length, inner_width = inner_act.shape
    heads = step_raw.shape[1]
    groups, state_dim = state_write.shape[1:]
    per_group = heads // groups
    head_dim = inner_width // heads
    group_width = per_group * head_dim
    write_width = groups * state_dim
    n_sp = lax.axis_size("sp")
    place = lax.axis_index("sp")
    writes = state_write.reshape(length, write_width)
    reads = state_read.reshape(length, write_width)
    last = jnp.concatenate(
        [inner_act[length - HALO :], writes[length - HALO :], reads[length - HALO :]], axis=1
    )
    halo = lax.ppermute(last, "sp", [(i, i + 1) for i in range(n_sp - 1)])

    step_len = jax.nn.softplus(step_raw.astype(F32) + step_bias[None, :])
    rate = -jnp.exp(decay_log)
    lower = jnp.tril(jnp.ones((length, length), F32))
    cumul = jnp.dot(lower, step_len * rate[None, :], precision=HIGH)
    total = cumul[-1]
    to_end = jnp.exp(total[None, :] - cumul) * step_len
    by_group = lambda a: a.reshape(length, groups, per_group).transpose(1, 0, 2)
    cum_g = by_group(cumul)
    cum_t = cum_g.transpose(0, 2, 1)
    step_t = by_group(step_len).transpose(0, 2, 1)
    end_g = by_group(to_end)

    col = lambda rows, cols: pl.BlockSpec((rows, cols), lambda g: (0, g))
    lead = lambda a: pl.BlockSpec((1,) + a.shape[1:], lambda g: (g, 0, 0))
    taps = conv_inner.shape[0]
    params = pltpu.CompilerParams(vmem_limit_bytes=48 * 2**20)
    xs, bw, cr, state = pl.pallas_call(
        functools.partial(conv_kernel, per_group),
        grid=(groups,),
        out_shape=(
            jax.ShapeDtypeStruct((length, inner_width), BF16),
            jax.ShapeDtypeStruct((length, write_width), BF16),
            jax.ShapeDtypeStruct((length, write_width), BF16),
            jax.ShapeDtypeStruct((groups * group_width, state_dim), BF16),
        ),
        in_specs=[
            col(length, group_width), col(length, state_dim), col(length, state_dim),
            col(HALO, group_width), col(HALO, state_dim), col(HALO, state_dim),
            col(taps, group_width), col(taps, state_dim), col(taps, state_dim), lead(end_g),
        ],
        out_specs=(
            col(length, group_width), col(length, state_dim), col(length, state_dim),
            pl.BlockSpec((group_width, state_dim), lambda g: (g, 0)),
        ),
        scratch_shapes=[pltpu.VMEM((length + HALO, max(group_width, state_dim)), F32)],
        compiler_params=params,
        cost_estimate=pl.CostEstimate(flops=10**9, bytes_accessed=10**7, transcendentals=10**6),
    )(
        inner_act, writes, reads,
        halo[:, :inner_width], halo[:, inner_width : inner_width + write_width],
        halo[:, inner_width + write_width :],
        conv_inner, conv_write.reshape(taps, write_width), conv_read.reshape(taps, write_width), end_g,
    )
    states = lax.all_gather(state, "sp")
    totals = lax.all_gather(total, "sp")

    inside = pl.pallas_call(
        functools.partial(inside_kernel, per_group),
        grid=(groups,),
        out_shape=jax.ShapeDtypeStruct((length, inner_width), F32),
        in_specs=[
            col(length, group_width), col(length, state_dim), col(length, state_dim),
            lead(cum_g), lead(cum_t), lead(step_t),
        ],
        out_specs=col(length, group_width),
        compiler_params=params,
        cost_estimate=pl.CostEstimate(
            flops=4 * 10**9, bytes_accessed=10**7, transcendentals=3 * 10**6
        ),
    )(xs, bw, cr, cum_g, cum_t, step_t)

    order = jnp.arange(n_sp)
    between = ((order[None, :] > order[:, None]) & (order[None, :] < place)).astype(F32)
    left = jnp.exp(jnp.sum(between[:, :, None] * totals[None], axis=1))
    left = jnp.where((order < place)[:, None], left, 0.0)
    left = jnp.repeat(left, head_dim, axis=1)
    arriving = jnp.sum(left[:, :, None] * states.astype(F32), axis=0).astype(BF16)

    mixed_inner = pl.pallas_call(
        functools.partial(outside_kernel, per_group),
        grid=(groups,),
        out_shape=jax.ShapeDtypeStruct((length, inner_width), BF16),
        in_specs=[
            col(length, group_width), col(length, state_dim),
            pl.BlockSpec((group_width, state_dim), lambda g: (g, 0)),
            lead(cum_g), col(length, group_width), col(1, group_width),
        ],
        out_specs=col(length, group_width),
        compiler_params=params,
        cost_estimate=pl.CostEstimate(flops=10**9, bytes_accessed=10**7, transcendentals=10**6),
    )(inside, cr, arriving, cum_g, gate_act, inner_gain[None, :])

    partial_value = jnp.dot(mixed_inner, out_weight, preferred_element_type=F32)
    full_width = partial_value.shape[1]
    local_experts = expert_gate.shape[0]
    expert_count = local_experts * n_sp
    ids = expert_ids.reshape(-1)
    onehot = (ids[:, None] == jnp.arange(expert_count, dtype=jnp.int32)[None, :]).astype(BF16)
    pairs = ids.shape[0]
    before = jnp.tril(jnp.ones((pairs, pairs), BF16), -1)
    earlier = jnp.dot(before, onehot, preferred_element_type=F32)
    slot_of = jnp.sum(earlier * onehot.astype(F32), axis=1).astype(jnp.int32)
    target = (ids * CAP + slot_of).reshape(length, TOPK)
    slots = jnp.arange(expert_count * CAP, dtype=jnp.int32)
    named = [target[:, k][:, None] == slots[None, :] for k in range(TOPK)]
    place_of = functools.reduce(jnp.logical_or, named).astype(BF16)
    mix = functools.reduce(
        jnp.add, [jnp.where(n, expert_weights[:, k : k + 1], 0.0) for k, n in enumerate(named)]
    )
    mix_high = mix.astype(BF16)
    mix_low = (mix - mix_high.astype(F32)).astype(BF16)

    out_width = expert_down.shape[2]
    own_start = lax.axis_index("tp") * out_width
    projected = lax.psum_scatter(
        partial_value.astype(BF16), "tp", scatter_dimension=1, tiled=True
    ).astype(F32)
    kept = lax.dynamic_slice_in_dim(stream, own_start, out_width, 1).astype(F32) + projected
    square_total = lax.psum(jnp.sum(kept * kept, axis=1), "tp")
    gain_share = lax.dynamic_slice_in_dim(ffn_gain, own_start, out_width, 0)
    scale_rows = lax.rsqrt(square_total / full_width + EPS)
    normed = (kept * scale_rows[:, None] * gain_share[None, :]).astype(BF16)
    outgoing = tn_dot(place_of, normed).astype(BF16)
    back = run_experts(
        outgoing.reshape(n_sp, local_experts, CAP, out_width), expert_gate, expert_up, expert_down
    )
    results = back.reshape(expert_count * CAP, out_width)
    moe = jnp.dot(mix_high, results, preferred_element_type=F32) + jnp.dot(
        mix_low, results, preferred_element_type=F32
    )
    return (kept + moe).astype(BF16)


def solution(mesh):
    return jax.shard_map(
        per_device,
        mesh=mesh,
        in_specs=(
            P("sp", None), P("sp", "tp"), P("sp", "tp"), P("sp", "tp", None), P("sp", "tp", None),
            P("sp", "tp"), P(None, "tp"), P(None, "tp", None), P(None, "tp", None), P("tp"), P("tp"),
            P("tp"), P("tp", None), P(), P("sp", None), P("sp", None), P("sp", None, "tp"),
            P("sp", None, "tp"), P("sp", None, "tp"),
        ),
        out_specs=P("sp", "tp"),
        check_vma=False,
    )
```

profile of v0, /device:TPU:9, one launch (start us, length us, event | category | flops | bytes accessed | tf_op | source)
XLA Modules:
  0.0 234.8 jit_solution(2669456826311113155)
XLA Ops:
  6.6 0.8 slice_bitcast_fusion.1
  7.4 0.7 slice_bitcast_fusion
  8.1 0.7 slice.39
  8.8 3.8 %collective-permute-start = (bf16[8,2048]{1,0:T(8,128)(2,1)S(1)}, bf16[8,2048]{1,0:T(8,128)(2,1)S(1)}, u32[]{:S(2)}, u32[]{:S(2)}) collective-permute-start(bf16[8,2048]{1,0:T(8,128)(2,1)S(1)} %pad_maximum_fusion), channel_id=1, source_target_pairs={{0,4},{4,8},{8,12},{12,16},{16,20},{20,24},{24,28},{1,5},{5,9},{9,... | collective-permute-start | bytes 98312 | tf_op jit(solution)/shard_map/ppermute | solution.py:366
  12.6 0.7 exponential_negate_fusion
  13.2 1.3 fusion.28
  14.5 0.2 slice_reduce_fusion
  14.7 0.8 compare_select_fusion
  15.5 1.2 copy_bitcast_fusion
  16.8 0.3 copy.41
  17.1 5.5 %shard_map.181 = (bf16[384,1024]{1,0:T(8,128)(2,1)S(1)}, bf16[384,512]{1,0:T(8,128)(2,1)S(1)}, bf16[384,512]{1,0:T(8,128)(2,1)S(1)}, bf16[1024,128]{1,0:T(8,128)(2,1)}) custom-call(bf16[384,1024]{1,0:T(8,128)(2,1)S(1)} %copy-done.2, bf16[384,512]{1,0:T(8,128)(2,1)S(1)} %get-tuple-element.24.w_ref, bf16[384,512]{1,0:T(8,128)(2,1)S(1)} %get-tuple-element.23.r_ref, ...), custom_call_target="tpu_custom_call" | custom-call | flops 1000000000 | bytes 10000000 | tf_op jit(solution)/shard_map/pallas_call | solution.py:384
  22.6 0.9 copy-done.4
  23.7 7.7 %all-gather.1 = f32[8,1,16]{2,1,0:T(1,128)S(1)} all-gather(f32[1,1,16]{2,1,0:T(1,128)S(1)} %bitcast.51), channel_id=1, replica_groups=mesh['sp'=8,'tp'=4] {'sp'}, dimensions={0}, use_global_device_ids=true | all-gather | bytes 576 | tf_op jit(solution)/shard_map/all_gather | solution.py:412
  31.6 0.7 mul.73
  32.3 0.3 copy.42
  32.6 1.1 copy-done.5
  33.8 3.8 %shard_map.182.in_ref = f32[384,1024]{1,0:T(8,128)S(1)} custom-call(bf16[384,1024]{1,0:T(8,128)(2,1)S(1)} %copy-done.5, bf16[384,512]{1,0:T(8,128)(2,1)S(1)} %get-tuple-element.10.bw_ref, bf16[384,512]{1,0:T(8,128)(2,1)S(1)} %get-tuple-element.11.cr_ref, f32[4,384,4]{2,1,0:T(8,128)S(1)} %bitcast.41, f32[4,4,384]{2,1,0:T(4,128)S(1)} %bitcast.44, ...), custom_call_target="tpu_custom_call" | custom-call | flops 4000000000 | bytes 10000000 | tf_op jit(solution)/shard_map/pallas_call | solution.py:414
  37.6 15.3 %all-gather.4.cloned.1.call-done = bf16[8192,128]{1,0:T(8,128)(2,1)} async-done(((bf16[1024,128]{1,0:T(8,128)(2,1)}), bf16[8192,128]{1,0:T(8,128)(2,1)}) %all-gather.4.cloned.1.call-update) | async-done | bytes 2097168 | tf_op jit(solution)/shard_map/all_gather | solution.py:411
  52.9 2.5 %fusion.state_ref = bf16[1024,128]{1,0:T(8,128)(2,1)S(1)} fusion(bf16[8,1024,128]{2,1,0:T(8,128)(2,1)} %bitcast.47, f32[8,1024]{1,0:T(8,128)} %mul.73), kind=kLoop, calls=%fused_computation.1 | loop fusion | flops 3014656 | bytes 2392064 | tf_op jit(solution)/shard_map/reduce_sum | solution.py:434
  55.4 4.8 %shard_map.183 = bf16[384,1024]{1,0:T(8,128)(2,1)S(1)} custom-call(f32[384,1024]{1,0:T(8,128)S(1)} %shard_map.182.in_ref, bf16[384,512]{1,0:T(8,128)(2,1)S(1)} %get-tuple-element.11.cr_ref, bf16[1024,128]{1,0:T(8,128)(2,1)S(1)} %fusion.state_ref, f32[4,384,4]{2,1,0:T(8,128)S(1)} %bitcast.42, bf16[384,1024]{1,0:T(8,128)(2,1)S(1)} %copy-done, ...), custom_call_target="tpu_custom_call" | custom-call | flops 1000000000 | bytes 10000000 | tf_op jit(solution)/shard_map/pallas_call | solution.py:436
  60.3 2.9 %convolution_convert_fusion.1 = bf16[384,2048]{1,0:T(8,128)(2,1)} fusion(bf16[384,1024]{1,0:T(8,128)(2,1)S(1)} %shard_map.183, bf16[1024,2048]{1,0:T(8,128)(2,1)S(1)} %copy-done.12), kind=kOutput, calls=%fused_computation.3 | convolution fusion | flops 1611399168 | bytes 6553600 | tf_op jit(solution)/shard_map/dot_general | solution.py:450
  63.4 0.1 eq.45
  63.6 0.6 fusion.20
  64.2 0.2 convert_element_type.67
  64.4 0.8 dynamic_slice.7
  65.3 28.1 %reduce-scatter.2.cloned.1.call-done = bf16[384,512]{1,0:T(8,128)(2,1)} async-done(((bf16[384,2048]{1,0:T(8,128)(2,1)}), bf16[384,512]{1,0:T(8,128)(2,1)}) %reduce-scatter.2.cloned.1.call-update) | async-done | bytes 393232 | tf_op jit(solution)/shard_map/reduce_scatter | solution.py:472
  93.4 1.2 multiply_reduce_fusion
  94.6 7.1 %psum.7 = f32[384]{0:T(512)S(1)} all-reduce(f32[384]{0:T(512)S(1)} %multiply_reduce_fusion), channel_id=1, replica_groups=mesh['sp'=8,'tp'=4] {'tp'}, use_global_device_ids=true, to_apply=%region_5.6 | all-reduce | flops 384 | bytes 3072 | tf_op jit(solution)/shard_map/psum | solution.py:476
  101.7 3.4 %convolution_convert_fusion = bf16[1536,512]{1,0:T(8,128)(2,1)} fusion(s32[384]{0:T(512)S(1)} %get-tuple-element.16, s32[384]{0:T(512)S(1)} %get-tuple-element.15, bf16[384,512]{1,0:T(8,128)(2,1)} %reduce-scatter.2.cloned.1.call-done, f32[512]{0:T(512)S(1)} %dynamic_slice.7, f32[384]{0:T(512)S(1)} %add_rsqrt_fusion, bf16[384,2048]{1,0:T(8,128)(2,1)S(1)} %copy-done.7, ...), kind=kOutput, calls=%fused_computation.2 | convolution fusion | flops 607715328 | bytes 2367492 | tf_op jit(solution)/shard_map/dot_general | solution.py:31
  105.1 118.5 %shard_map.184 = bf16[8,4,48,512]{3,2,1,0:T(8,128)(2,1)} custom-call(bf16[8,4,48,512]{3,2,1,0:T(8,128)(2,1)} %bitcast.56, bf16[4,2048,256]{2,1,0:T(8,128)(2,1)} %gate_hbm.1, bf16[4,2048,256]{2,1,0:T(8,128)(2,1)} %up_hbm.1, bf16[4,1024,512]{2,1,0:T(8,128)(2,1)} %down_hbm.1), custom_call_target="tpu_custom_call" | custom-call | flops 10000000000 | bytes 20000000 | tf_op jit(solution)/shard_map/pallas_call | solution.py:322
  223.6 2.5 %fusion.24 = f32[384,512]{1,0:T(8,128)S(1)} fusion(bf16[1536,512]{1,0:T(8,128)(2,1)} %bitcast.54, f32[384]{0:T(512)S(1)} %get-tuple-element.14, s32[384]{0:T(512)S(1)} %get-tuple-element.16, f32[384]{0:T(512)S(1)} %get-tuple-element.13, s32[384]{0:T(512)S(1)} %get-tuple-element.15), kind=kOutput, calls=%fused_computation.26 | convolution fusion | flops 607518720 | bytes 2365440 | tf_op jit(solution)/shard_map/dot_general | solution.py:485
  226.1 1.8 fusion.6
  (52 shorter events, 0.8 us)
Async XLA Ops:
  6.5 10.6 %copy-start.2 = (bf16[384,1024]{1,0:T(8,128)(2,1)S(1)}, bf16[384,1024]{1,0:T(8,128)(2,1)}, u32[]{:S(2)}) copy-start(bf16[384,1024]{1,0:T(8,128)(2,1)} %x_ref.1) | copy-start | bytes 2359300
  6.5 10.2 %copy-start.9 = (bf16[4,4,128]{2,1,0:T(4,128)(2,1)S(1)}, bf16[4,4,128]{2,1,0:T(4,128)(2,1)}, u32[]{:S(2)}) copy-start(bf16[4,4,128]{2,1,0:T(4,128)(2,1)} %param.27) | copy-start | bytes 12292
  6.5 10.2 %copy-start.10 = (bf16[4,4,128]{2,1,0:T(4,128)(2,1)S(1)}, bf16[4,4,128]{2,1,0:T(4,128)(2,1)}, u32[]{:S(2)}) copy-start(bf16[4,4,128]{2,1,0:T(4,128)(2,1)} %param.26) | copy-start | bytes 12292
  6.5 10.6 %copy-start.3 = (bf16[4,1024]{1,0:T(4,128)(2,1)S(1)}, bf16[4,1024]{1,0:T(4,128)(2,1)}, u32[]{:S(2)}) copy-start(bf16[4,1024]{1,0:T(4,128)(2,1)} %kx_ref.1) | copy-start | bytes 24580
  6.5 46.3 %all-gather.4.cloned.1.call-start = ((), (), s32[]{:S(2)}) async-start(), calls=%async_computation.2 | async-start | bytes 2359296 | tf_op jit(solution)/shard_map/all_gather | solution.py:411
  8.8 8.3 %collective-permute-start = (bf16[8,2048]{1,0:T(8,128)(2,1)S(1)}, bf16[8,2048]{1,0:T(8,128)(2,1)S(1)}, u32[]{:S(2)}, u32[]{:S(2)}) collective-permute-start(bf16[8,2048]{1,0:T(8,128)(2,1)S(1)} %pad_maximum_fusion), channel_id=1, source_target_pairs={{0,4},{4,8},{8,12},{12,16},{16,20},{20,24},{24,28},{1,5},{5,9},{9,... | collective-permute-start | bytes 98312 | tf_op jit(solution)/shard_map/ppermute | solution.py:366
  22.6 0.9 copy-start.4
  23.6 69.8 %reduce-scatter.2.cloned.1.call-start = ((), (), s32[]{:S(2)}) async-start(), calls=%async_computation.1 | async-start | bytes 1966080 | tf_op jit(solution)/shard_map/reduce_scatter | solution.py:472
  32.6 1.1 copy-start.5
  37.5 17.9 %copy-start = (bf16[384,1024]{1,0:T(8,128)(2,1)S(1)}, bf16[384,1024]{1,0:T(8,128)(2,1)}, u32[]{:S(2)}) copy-start(bf16[384,1024]{1,0:T(8,128)(2,1)} %gate_ref.1) | copy-start | bytes 2359300
  37.5 17.9 %copy-start.1 = (f32[1024]{0:T(1024)S(1)}, f32[1024]{0:T(1024)}, u32[]{:S(2)}) copy-start(f32[1024]{0:T(1024)} %param.30) | copy-start | bytes 12292
  55.4 4.8 %copy-start.12 = (bf16[1024,2048]{1,0:T(8,128)(2,1)S(1)}, bf16[1024,2048]{1,0:T(8,128)(2,1)}, u32[]{:S(2)}) copy-start(bf16[1024,2048]{1,0:T(8,128)(2,1)} %param.31) | copy-start | bytes 12582916
  60.3 3.0 %copy-start.8 = (s32[384,2]{0,1:T(2,128)S(1)}, s32[384,2]{0,1:T(2,128)}, u32[]{:S(2)}) copy-start(s32[384,2]{0,1:T(2,128)} %param.33) | copy-start | bytes 9220
  63.2 2.0 copy-start.11
  63.2 30.2 %copy-start.7 = (bf16[384,2048]{1,0:T(8,128)(2,1)S(1)}, bf16[384,2048]{1,0:T(8,128)(2,1)}, u32[]{:S(2)}) copy-start(bf16[384,2048]{1,0:T(8,128)(2,1)} %param.19) | copy-start | bytes 4718596
  223.6 2.5 %copy-start.6 = (bf16[384,512]{1,0:T(8,128)(2,1)S(1)}, bf16[384,512]{1,0:T(8,128)(2,1)}, u32[]{:S(2)}) copy-start(bf16[384,512]{1,0:T(8,128)(2,1)} %reduce-scatter.2.cloned.1.call-done) | copy-start | bytes 1179652
  223.6 2.5 %copy-start.13 = (bf16[8,4,48,512]{3,2,1,0:T(8,128)(2,1)S(1)}, bf16[8,4,48,512]{3,2,1,0:T(8,128)(2,1)}, u32[]{:S(2)}) copy-start(bf16[8,4,48,512]{3,2,1,0:T(8,128)(2,1)} %shard_map.184) | copy-start | bytes 4718596
Sparse Core Ops, SparseCore 0:
  23.7 29.1 all-gather.3
  63.4 29.9 reduce-scatter.1
where the time goes:
time: 235 us
  Pallas kernels  133 us (57%)
  waiting for transfers between devices  43.4 us (18%)
  blocking collectives  14.8 us (6%)
  between operations  13.8 us (6%)
  matrix products  12.5 us (5%)
  local copies, waits for them, and re-layouts  8.48 us (4%)
  other arithmetic  5.4 us (2%)
  starting transfers between devices  3.84 us (2%)
    pallas_call x1, Pallas kernels, run_experts(): pl.pallas_call(functools.partial(experts_kernel, n_sp, n_tp), out_shape=j...  118 us
    reduce_scatter x1, waiting for transfers between devices, per_device(): lax.psum_scatter(partial_value.astype(BF16), 'tp', scatter_dimension=1, t...  28.1 us
    all_gather x1, waiting for transfers between devices, per_device(): states = lax.all_gather(state, 'sp')  15.3 us
    all_gather x1, blocking collectives, per_device(): totals = lax.all_gather(total, 'sp')  7.72 us
    psum x1, blocking collectives, per_device(): square_total = lax.psum(jnp.sum(kept * kept, axis=1), 'tp')  7.1 us
    pallas_call x1, Pallas kernels, per_device(): pl.pallas_call(functools.partial(conv_kernel, per_group), grid=(groups,),...  5.5 us
    pallas_call x1, Pallas kernels, per_device(): pl.pallas_call(functools.partial(outside_kernel, per_group), grid=(groups...  4.8 us
  transfers between devices with their start and end apart: 3, of which 2 were waited for; matrix products, arithmetic and copies ran while one was open for 3% of the time, Pallas kernels for 2%

commit v1 on v0

--- a/solution.py
+++ b/solution.py
@@ -32,7 +32,7 @@
 
 
 def conv_kernel(
-    per_group, x_ref, w_ref, r_ref, hx_ref, hw_ref, hr_ref, kx_ref, kw_ref, kr_ref, end_ref,
+    per_group, x_ref, w_ref, r_ref, hx_ref, hw_ref, hr_ref, kx_ref, kw_ref, kr_ref, end_ref, sum_ref,
     xs_ref, bw_ref, cr_ref, state_ref, pad_ref,
 ):
     length = x_ref.shape[0]
@@ -59,7 +59,15 @@
         xs[:, h * head_dim : (h + 1) * head_dim] * end_ref[0, :, h : h + 1] for h in range(per_group)
     ]
     weighted = jnp.concatenate(scaled, axis=1).astype(BF16)
-    state_ref[...] = tn_dot(weighted, bw).astype(BF16)
+    state_ref[0, 0 : xs.shape[1], :] = tn_dot(weighted, bw).astype(BF16)
+    terms = []
+    rest = [jnp.broadcast_to(sum_ref[0, :, h : h + 1], (1, bw.shape[1])) for h in range(per_group)]
+    for _ in range(3):
+        cut = [r.astype(BF16).astype(F32) for r in rest]
+        terms += cut
+        rest = [r - c for r, c in zip(rest, cut)]
+    blank = jnp.zeros((state_ref.shape[1] - xs.shape[1] - len(terms), bw.shape[1]), F32)
+    state_ref[0, xs.shape[1] :, :] = jnp.concatenate(terms + [blank], axis=0).astype(BF16)
 
 
 def inside_kernel(per_group, xs_ref, bw_ref, cr_ref, cum_ref, cumt_ref, stept_ref, out_ref):
@@ -86,7 +94,20 @@
     per_group, in_ref, cr_ref, state_ref, cum_ref, gate_ref, gain_ref, out_ref
 ):
     head_dim = in_ref.shape[1] // per_group
-    outside = nt_dot(cr_ref[...], state_ref[...])
+    width = in_ref.shape[1]
+    place = lax.axis_index("sp")
+    entering = []
+    for h in range(per_group):
+        cut = slice(h * head_dim, (h + 1) * head_dim)
+        held = jnp.zeros((head_dim, state_ref.shape[3]), F32)
+        for j in range(state_ref.shape[0]):
+            tail = state_ref[j, 0, width:, :].astype(F32)
+            total = sum(tail[i * per_group + h : i * per_group + h + 1, :] for i in range(3))
+            later = held * jnp.exp(total) + state_ref[j, 0, cut, :].astype(F32)
+            held = jnp.where(j < place, later, held)
+        entering.append(held)
+    arriving = jnp.concatenate(entering, axis=0).astype(BF16)
+    outside = nt_dot(cr_ref[...], arriving)
     gates = silu(gate_ref[...].astype(F32))
     pieces = []
     for h in range(per_group):
@@ -96,6 +117,123 @@
         scale = lax.rsqrt(jnp.mean(part * part, axis=1, keepdims=True) + EPS)
         pieces.append(part * scale)
     out_ref[...] = (jnp.concatenate(pieces, axis=1) * gain_ref[...]).astype(BF16)
+
+
+def project_kernel(
+    mixed_ref, weight_ref, stream_ref, gain_ref, place_ref, kept_ref, slots_ref,
+    part_ref, got_ref, hop_ref, square_ref, squares_ref,
+    n_send, n_recv, h_send, h_recv, f_send, f_recv, q_send, q_recv,
+):
+    me = lax.axis_index("sp")
+    tp = lax.axis_index("tp")
+    xp = tp + 1 - 2 * (tp % 2)
+    yp = (tp + 2) % 4
+    dp = (xp + 2) % 4
+    length, share = kept_ref.shape
+    half = length // 2
+
+    barrier = pltpu.get_barrier_semaphore()
+    for peer in (xp, yp, dp):
+        pl.semaphore_signal(barrier, inc=1, device_id=(me, peer), device_id_type=MESH)
+    pl.semaphore_wait(barrier, 3)
+
+    def remote(src, dst, send, recv, peer):
+        return pltpu.make_async_remote_copy(
+            src_ref=src, dst_ref=dst, send_sem=send, recv_sem=recv,
+            device_id=(me, peer), device_id_type=MESH,
+        )
+
+    def term(q):
+        columns = pl.ds(pl.multiple_of(q * share, share), share)
+        return jnp.dot(mixed_ref[...], weight_ref[:, columns], preferred_element_type=F32).astype(BF16)
+
+    part_ref[2] = term(dp)
+    first, second = pl.ds(0, half), pl.ds(half, half)
+    hops = [
+        remote(part_ref.at[2, first], hop_ref.at[0], h_send.at[0], h_recv.at[0], xp),
+        remote(part_ref.at[2, second], hop_ref.at[1], h_send.at[1], h_recv.at[1], yp),
+    ]
+    for copy in hops:
+        copy.start()
+    near = []
+    for i, peer in enumerate((xp, yp)):
+        part_ref[i] = term(peer)
+        copy = remote(part_ref.at[i], got_ref.at[i], n_send.at[i], n_recv.at[i], peer)
+        copy.start()
+        near.append(copy)
+    kept = stream_ref[...].astype(F32) + term(tp).astype(F32)
+    passed = [
+        remote(hop_ref.at[0], got_ref.at[2, first], f_send.at[0], f_recv.at[0], yp),
+        remote(hop_ref.at[1], got_ref.at[2, second], f_send.at[1], f_recv.at[1], xp),
+    ]
+    for hop, copy in zip(hops, passed):
+        hop.wait_recv()
+        copy.start()
+    for copy in near + passed:
+        copy.wait_recv()
+    for i in range(3):
+        kept = kept + got_ref[i].astype(F32)
+    kept_ref[...] = kept
+    ones = jnp.ones((8, share), F32)
+    square_ref[...] = lax.dot_general(
+        ones, kept * kept, (((1,), (1,)), ((), ())), precision=HIGH, preferred_element_type=F32
+    )
+    asks = []
+    for i, peer in enumerate((xp, yp, dp)):
+        copy = remote(square_ref, squares_ref.at[i], q_send.at[i], q_recv.at[i], peer)
+        copy.start()
+        asks.append(copy)
+    for copy in asks:
+        copy.wait_recv()
+    squares = square_ref[...] + squares_ref[0] + squares_ref[1] + squares_ref[2]
+    scale = lax.rsqrt(squares / weight_ref.shape[1] + EPS)
+    pick = jnp.full((8, share), 0.125, F32)
+    spread = lax.dot_general(
+        scale, pick, (((0,), (0,)), ((), ())), precision=HIGH, preferred_element_type=F32
+    )
+    normed = (kept * spread * gain_ref[...]).astype(BF16)
+    for i in range(slots_ref.shape[0]):
+        slots_ref[i] = jnp.dot(place_ref[i], normed, preferred_element_type=F32).astype(BF16)
+    for copy in hops + near + passed + asks:
+        copy.wait_send()
+
+
+def run_project(mixed, weight, stream_share, gain_share, place_of):
+    n_tp = lax.axis_size("tp")
+    length, share = stream_share.shape
+    if n_tp != 4 or length % 32:
+        partial_value = jnp.dot(mixed, weight, preferred_element_type=F32).astype(BF16)
+        projected = lax.psum_scatter(partial_value, "tp", scatter_dimension=1, tiled=True)
+        kept = stream_share.astype(F32) + projected.astype(F32)
+        squares = lax.psum(jnp.sum(kept * kept, axis=1), "tp")
+        scale = lax.rsqrt(squares / weight.shape[1] + EPS)
+        normed = (kept * scale[:, None] * gain_share[None, :]).astype(BF16)
+        slots = jnp.einsum("ist,td->isd", place_of, normed, preferred_element_type=F32)
+        return kept, slots.astype(BF16)
+    dma = lambda count: pltpu.SemaphoreType.DMA((count,))
+    return pl.pallas_call(
+        project_kernel,
+        out_shape=(
+            jax.ShapeDtypeStruct((length, share), F32),
+            jax.ShapeDtypeStruct(place_of.shape[:2] + (share,), BF16),
+        ),
+        in_specs=[VMEM] * 5,
+        out_specs=(VMEM, VMEM),
+        scratch_shapes=[
+            pltpu.VMEM((3, length, share), BF16),
+            pltpu.VMEM((3, length, share), BF16),
+            pltpu.VMEM((2, length // 2, share), BF16),
+            pltpu.VMEM((8, length), F32),
+            pltpu.VMEM((3, 8, length), F32),
+            dma(2), dma(2), dma(2), dma(2), dma(2), dma(2), dma(3), dma(3),
+        ],
+        compiler_params=pltpu.CompilerParams(
+            collective_id=1, has_side_effects=True, vmem_limit_bytes=48 * 2**20
+        ),
+        cost_estimate=pl.CostEstimate(
+            flops=4 * 10**9, bytes_accessed=10**7, transcendentals=10**4
+        ),
+    )(mixed, weight, stream_share, gain_share[None, :], place_of)
 
 
 def experts_kernel(
@@ -357,7 +495,6 @@
     group_width = per_group * head_dim
     write_width = groups * state_dim
     n_sp = lax.axis_size("sp")
-    place = lax.axis_index("sp")
     writes = state_write.reshape(length, write_width)
     reads = state_read.reshape(length, write_width)
     last = jnp.concatenate(
@@ -376,6 +513,8 @@
     cum_t = cum_g.transpose(0, 2, 1)
     step_t = by_group(step_len).transpose(0, 2, 1)
     end_g = by_group(to_end)
+    sum_g = total.reshape(groups, 1, per_group)
+    state_rows = group_width + -(-3 * per_group // 16) * 16
 
     col = lambda rows, cols: pl.BlockSpec((rows, cols), lambda g: (0, g))
     lead = lambda a: pl.BlockSpec((1,) + a.shape[1:], lambda g: (g, 0, 0))
@@ -388,16 +527,17 @@
             jax.ShapeDtypeStruct((length, inner_width), BF16),
             jax.ShapeDtypeStruct((length, write_width), BF16),
             jax.ShapeDtypeStruct((length, write_width), BF16),
-            jax.ShapeDtypeStruct((groups * group_width, state_dim), BF16),
+            jax.ShapeDtypeStruct((groups, state_rows, state_dim), BF16),
         ),
         in_specs=[
             col(length, group_width), col(length, state_dim), col(length, state_dim),
             col(HALO, group_width), col(HALO, state_dim), col(HALO, state_dim),
             col(taps, group_width), col(taps, state_dim), col(taps, state_dim), lead(end_g),
+            lead(sum_g),
         ],
         out_specs=(
             col(length, group_width), col(length, state_dim), col(length, state_dim),
-            pl.BlockSpec((group_width, state_dim), lambda g: (g, 0)),
+            pl.BlockSpec((1, state_rows, state_dim), lambda g: (g, 0, 0)),
         ),
         scratch_shapes=[pltpu.VMEM((length + HALO, max(group_width, state_dim)), F32)],
         compiler_params=params,
@@ -406,10 +546,9 @@
         inner_act, writes, reads,
         halo[:, :inner_width], halo[:, inner_width : inner_width + write_width],
         halo[:, inner_width + write_width :],
-        conv_inner, conv_write.reshape(taps, write_width), conv_read.reshape(taps, write_width), end_g,
+        conv_inner, conv_write.reshape(taps, write_width), conv_read.reshape(taps, write_width), end_g, sum_g,
     )
     states = lax.all_gather(state, "sp")
-    totals = lax.all_gather(total, "sp")
 
     inside = pl.pallas_call(
         functools.partial(inside_kernel, per_group),
@@ -426,29 +565,20 @@
         ),
     )(xs, bw, cr, cum_g, cum_t, step_t)
 
-    order = jnp.arange(n_sp)
-    between = ((order[None, :] > order[:, None]) & (order[None, :] < place)).astype(F32)
-    left = jnp.exp(jnp.sum(between[:, :, None] * totals[None], axis=1))
-    left = jnp.where((order < place)[:, None], left, 0.0)
-    left = jnp.repeat(left, head_dim, axis=1)
-    arriving = jnp.sum(left[:, :, None] * states.astype(F32), axis=0).astype(BF16)
-
     mixed_inner = pl.pallas_call(
         functools.partial(outside_kernel, per_group),
         grid=(groups,),
         out_shape=jax.ShapeDtypeStruct((length, inner_width), BF16),
         in_specs=[
             col(length, group_width), col(length, state_dim),
-            pl.BlockSpec((group_width, state_dim), lambda g: (g, 0)),
+            pl.BlockSpec((n_sp, 1, state_rows, state_dim), lambda g: (0, g, 0, 0)),
             lead(cum_g), col(length, group_width), col(1, group_width),
         ],
         out_specs=col(length, group_width),
         compiler_params=params,
         cost_estimate=pl.CostEstimate(flops=10**9, bytes_accessed=10**7, transcendentals=10**6),
-    )(inside, cr, arriving, cum_g, gate_act, inner_gain[None, :])
-
-    partial_value = jnp.dot(mixed_inner, out_weight, preferred_element_type=F32)
-    full_width = partial_value.shape[1]
+    )(inside, cr, states, cum_g, gate_act, inner_gain[None, :])
+
     local_experts = expert_gate.shape[0]
     expert_count = local_experts * n_sp
     ids = expert_ids.reshape(-1)
@@ -460,7 +590,8 @@
     target = (ids * CAP + slot_of).reshape(length, TOPK)
     slots = jnp.arange(expert_count * CAP, dtype=jnp.int32)
     named = [target[:, k][:, None] == slots[None, :] for k in range(TOPK)]
-    place_of = functools.reduce(jnp.logical_or, named).astype(BF16)
+    placed = [slots[:, None] == target[:, k][None, :] for k in range(TOPK)]
+    place_of = functools.reduce(jnp.logical_or, placed).astype(BF16)
     mix = functools.reduce(
         jnp.add, [jnp.where(n, expert_weights[:, k : k + 1], 0.0) for k, n in enumerate(named)]
     )
@@ -469,15 +600,11 @@
 
     out_width = expert_down.shape[2]
     own_start = lax.axis_index("tp") * out_width
-    projected = lax.psum_scatter(
-        partial_value.astype(BF16), "tp", scatter_dimension=1, tiled=True
-    ).astype(F32)
-    kept = lax.dynamic_slice_in_dim(stream, own_start, out_width, 1).astype(F32) + projected
-    square_total = lax.psum(jnp.sum(kept * kept, axis=1), "tp")
+    stream_share = lax.dynamic_slice_in_dim(stream, own_start, out_width, 1)
     gain_share = lax.dynamic_slice_in_dim(ffn_gain, own_start, out_width, 0)
-    scale_rows = lax.rsqrt(square_total / full_width + EPS)
-    normed = (kept * scale_rows[:, None] * gain_share[None, :]).astype(BF16)
-    outgoing = tn_dot(place_of, normed).astype(BF16)
+    kept, outgoing = run_project(
+        mixed_inner, out_weight, stream_share, gain_share, place_of.reshape(n_sp, -1, length)
+    )
     back = run_experts(
         outgoing.reshape(n_sp, local_experts, CAP, out_width), expert_gate, expert_up, expert_down
     )

time: 235 us -> 223 us (0.949)
  waiting for transfers between devices: 43.4 us -> 16.1 us
  Pallas kernels: 133 us -> 159 us
  blocking collectives: 14.8 us -> 0 us
  local copies, waits for them, and re-layouts: 8.48 us -> 21.7 us
  matrix products: 12.5 us -> 6.07 us
  other arithmetic: 5.4 us -> 1.87 us
    reduce_scatter x1 -> x0, waiting for transfers between devices: 28.1 us -> none  [per_device(): lax.psum_scatter(partial_value.astype(BF16), 'tp', scatter_dimension=1, t...]
    pallas_call x0 -> x1, Pallas kernels: none -> 27.6 us  [run_project(): pl.pallas_call(project_kernel, out_shape=(jax.ShapeDtypeStruct((length, s...]
    unnamed x31 -> x55, local copies, waits for them, and re-layouts: 3.71 us -> 15.6 us
    all_gather x1 -> x0, blocking collectives: 7.72 us -> none  [per_device(): totals = lax.all_gather(total, 'sp')]
    psum x1 -> x0, blocking collectives: 7.1 us -> none  [per_device(): square_total = lax.psum(jnp.sum(kept * kept, axis=1), 'tp')]
    dot_general x2 -> x0, matrix products: 6.36 us -> none  [the longest x1 3.42 us: tn_dot(): lax.dot_general(a, b, (((0,), (0,)), ((), ())), preferred_element_type=F32)]
    reduce_sum x3 -> x0, other arithmetic: 3.82 us -> none  [the longest x1 2.53 us: per_device(): jnp.sum(left[:, :, None] * states.astype(F32), axis=0).astype(BF16)]
    pallas_call x1, Pallas kernels: 118 us -> 116 us  [run_experts(): pl.pallas_call(functools.partial(experts_kernel, n_sp, n_tp), out_shape=j...]
  transfers between devices with their start and end apart: 3 -> 2, of which waited for: 2 -> 1; matrix products, arithmetic and copies ran while one was open for 3% -> 4% of each run, Pallas kernels for 2% -> 2%
where the time goes in v1:
time: 223 us; the launch traced here: 222 us
  Pallas kernels  159 us (71%)
  local copies, waits for them, and re-layouts  21.7 us (10%)
  waiting for transfers between devices  16.1 us (7%)
  between operations  13.7 us (6%)
  matrix products  6.07 us (3%)
  starting transfers between devices  3.8 us (2%)
    pallas_call x1, Pallas kernels, run_experts(): pl.pallas_call(functools.partial(experts_kernel, n_sp, n_tp), out_shape=j...  116 us
    pallas_call x1, Pallas kernels, run_project(): pl.pallas_call(project_kernel, out_shape=(jax.ShapeDtypeStruct((length, s...  27.6 us
    all_gather x1, waiting for transfers between devices, per_device(): states = lax.all_gather(state, 'sp')  16.1 us
    unnamed x55, local copies, waits for them, and re-layouts  15.6 us
    pallas_call x1, Pallas kernels, per_device(): pl.pallas_call(functools.partial(outside_kernel, per_group), grid=(groups...  6.22 us
    pallas_call x1, Pallas kernels, per_device(): pl.pallas_call(functools.partial(conv_kernel, per_group), grid=(groups,),...  5.28 us
  transfers between devices with their start and end apart: 2, of which 1 were waited for; matrix products, arithmetic and copies ran while one was open for 4% of the time, Pallas kernels for 2%

profile of v1, /device:TPU:9, one launch (start us, length us, event | category | flops | bytes accessed | tf_op | source)
XLA Modules:
  0.0 222.0 jit_solution(9646933798762064585)
XLA Ops:
  6.6 0.8 slice_bitcast_fusion
  7.4 0.7 slice_bitcast_fusion.1
  8.1 0.7 slice.41
  8.8 3.8 %collective-permute-start = (bf16[8,2048]{1,0:T(8,128)(2,1)S(1)}, bf16[8,2048]{1,0:T(8,128)(2,1)S(1)}, u32[]{:S(2)}, u32[]{:S(2)}) collective-permute-start(bf16[8,2048]{1,0:T(8,128)(2,1)S(1)} %pad_maximum_fusion), channel_id=1, source_target_pairs={{0,4},{4,8},{8,12},{12,16},{16,20},{20,24},{24,28},{1,5},{5,9},{9,... | collective-permute-start | bytes 98312 | tf_op jit(solution)/shard_map/ppermute | solution.py:503
  12.6 0.7 exponential_negate_fusion
  13.3 1.3 fusion.23
  14.7 0.8 compare_select_fusion
  15.5 1.2 copy_bitcast_fusion
  17.3 1.1 copy-done.12
  18.4 5.3 %shard_map.181 = (bf16[384,1024]{1,0:T(8,128)(2,1)S(1)}, bf16[384,512]{1,0:T(8,128)(2,1)S(1)}, bf16[384,512]{1,0:T(8,128)(2,1)S(1)}, bf16[4,272,128]{2,1,0:T(8,128)(2,1)}) custom-call(bf16[384,1024]{1,0:T(8,128)(2,1)S(1)} %copy-done.12, bf16[384,512]{1,0:T(8,128)(2,1)S(1)} %get-tuple-element.28.w_ref, bf16[384,512]{1,0:T(8,128)(2,1)S(1)} %get-tuple-element.27.r_ref, ...), custom_call_target="tpu_custom_call" | custom-call | flops 1000000000 | bytes 10000000 | tf_op jit(solution)/shard_map/pallas_call | solution.py:523
  23.7 0.7 copy-done.4
  24.4 0.9 copy-done.15
  25.3 0.7 copy-done.17
  28.2 0.8 dynamic_slice.7
  29.6 0.8 constant_dynamic-slice_fusion.stream_ref
  30.8 1.0 copy-done.5
  31.8 0.7 copy-done.9
  32.5 0.7 copy-done.10
  33.3 1.2 copy-done.16
  34.4 1.0 copy-done.18
  35.4 3.8 %shard_map.182.in_ref = f32[384,1024]{1,0:T(8,128)S(1)} custom-call(bf16[384,1024]{1,0:T(8,128)(2,1)S(1)} %copy-done.16, bf16[384,512]{1,0:T(8,128)(2,1)S(1)} %copy-done.18, bf16[384,512]{1,0:T(8,128)(2,1)S(1)} %copy-done.5, f32[4,384,4]{2,1,0:T(8,128)S(1)} %bitcast.38, f32[4,4,384]{2,1,0:T(4,128)S(1)} %bitcast.41, f32[4,4,384]{2,1,0:T(4,128)S(1)} %bitcast.42), custom_call_target="tpu_custom_call" | custom-call | flops 4000000000 | bytes 10000000 | tf_op jit(solution)/shard_map/pallas_call | solution.py:553
  39.2 1.1 copy-done.1
  40.3 16.1 %all-gather.3.cloned.1.call-done = bf16[32,272,128]{2,1,0:T(8,128)(2,1)} async-done(((bf16[4,272,128]{2,1,0:T(8,128)(2,1)}), bf16[32,272,128]{2,1,0:T(8,128)(2,1)}) %all-gather.3.cloned.1.call-update) | async-done | bytes 2228240 | tf_op jit(solution)/shard_map/all_gather | solution.py:551
  56.4 1.4 copy-done.2
  57.8 1.1 copy-done.3
  59.0 1.0 copy-done.6
  60.0 6.2 %shard_map.183.mixed_ref = bf16[384,1024]{1,0:T(8,128)(2,1)S(1)} custom-call(f32[384,1024]{1,0:T(8,128)S(1)} %copy-done.2, bf16[384,512]{1,0:T(8,128)(2,1)S(1)} %copy-done.6, bf16[8,4,272,128]{3,2,1,0:T(8,128)(2,1)} %bitcast.47, f32[4,384,4]{2,1,0:T(8,128)S(1)} %bitcast.39, bf16[384,1024]{1,0:T(8,128)(2,1)S(1)} %copy-done.3, f32[1,1024]{1,0:T(1,128)S(1)} %bitcast.43), custom_call_target="tpu_custom_call" | custom-call | flops 1000000000 | bytes 10000000 | tf_op jit(solution)/shard_map/pallas_call | solution.py:568
  66.2 27.6 %shard_map.184 = (f32[384,512]{1,0:T(8,128)S(1)}, bf16[8,192,512]{2,1,0:T(8,128)(2,1)S(1)}) custom-call(bf16[384,1024]{1,0:T(8,128)(2,1)S(1)} %shard_map.183.mixed_ref, bf16[1024,2048]{1,0:T(8,128)(2,1)} %weight_ref.1, bf16[384,512]{1,0:T(8,128)(2,1)S(1)} %copy-done.7, f32[1,512]{1,0:T(1,128)S(1)} %bitcast.45, bf16[8,192,384]{2,1,0:T(8,128)(2,1)S(1)} %or_convert_fusion.place_ref), custom_call_target="tpu_custom_call" | custom-call | flops 4000000000 | bytes 10000000 | tf_op jit(solution)/shard_map/pallas_call | solution.py:214
  93.9 1.1 copy-done.14
  95.0 115.9 %shard_map.185 = bf16[8,4,48,512]{3,2,1,0:T(8,128)(2,1)} custom-call(bf16[8,4,48,512]{3,2,1,0:T(8,128)(2,1)} %bitcast.46, bf16[4,2048,256]{2,1,0:T(8,128)(2,1)} %gate_hbm.1, bf16[4,2048,256]{2,1,0:T(8,128)(2,1)} %up_hbm.1, bf16[4,1024,512]{2,1,0:T(8,128)(2,1)} %down_hbm.1), custom_call_target="tpu_custom_call" | custom-call | flops 10000000000 | bytes 20000000 | tf_op jit(solution)/shard_map/pallas_call | solution.py:460
  210.9 2.5 %fusion.19 = f32[384,512]{1,0:T(8,128)S(1)} fusion(bf16[1536,512]{1,0:T(8,128)(2,1)} %bitcast.52, f32[384]{0:T(512)S(1)} %copy-done.24, s32[384]{0:T(512)S(1)} %get-tuple-element.20, f32[384]{0:T(512)S(1)} %copy-done.23, s32[384]{0:T(512)S(1)} %get-tuple-element.19), kind=kOutput, calls=%fused_computation.20 | convolution fusion | flops 607518720 | bytes 2365440 | tf_op jit(solution)/shard_map/dot_general | solution.py:612
  213.4 1.8 fusion.3
  (65 shorter events, 3.8 us)
Async XLA Ops:
  6.5 23.1 %copy-start = (bf16[384,2048]{1,0:T(8,128)(2,1)S(1)}, bf16[384,2048]{1,0:T(8,128)(2,1)}, u32[]{:S(2)}) copy-start(bf16[384,2048]{1,0:T(8,128)(2,1)} %param.19) | copy-start | bytes 4718596
  6.5 10.2 %copy-start.21 = (bf16[4,4,128]{2,1,0:T(4,128)(2,1)S(1)}, bf16[4,4,128]{2,1,0:T(4,128)(2,1)}, u32[]{:S(2)}) copy-start(bf16[4,4,128]{2,1,0:T(4,128)(2,1)} %param.26) | copy-start | bytes 12292
  6.5 10.2 %copy-start.20 = (bf16[4,4,128]{2,1,0:T(4,128)(2,1)S(1)}, bf16[4,4,128]{2,1,0:T(4,128)(2,1)}, u32[]{:S(2)}) copy-start(bf16[4,4,128]{2,1,0:T(4,128)(2,1)} %param.27) | copy-start | bytes 12292
  6.5 10.7 %copy-start.13 = (bf16[4,1024]{1,0:T(4,128)(2,1)S(1)}, bf16[4,1024]{1,0:T(4,128)(2,1)}, u32[]{:S(2)}) copy-start(bf16[4,1024]{1,0:T(4,128)(2,1)} %kx_ref.1) | copy-start | bytes 24580
  6.5 49.9 %all-gather.3.cloned.1.call-start = ((), (), s32[]{:S(2)}) async-start(), calls=%async_computation | async-start | bytes 2506752 | tf_op jit(solution)/shard_map/all_gather | solution.py:551
  8.8 8.4 %collective-permute-start = (bf16[8,2048]{1,0:T(8,128)(2,1)S(1)}, bf16[8,2048]{1,0:T(8,128)(2,1)S(1)}, u32[]{:S(2)}, u32[]{:S(2)}) collective-permute-start(bf16[8,2048]{1,0:T(8,128)(2,1)S(1)} %pad_maximum_fusion), channel_id=1, source_target_pairs={{0,4},{4,8},{8,12},{12,16},{16,20},{20,24},{24,28},{1,5},{5,9},{9,... | collective-permute-start | bytes 98312 | tf_op jit(solution)/shard_map/ppermute | solution.py:503
  17.2 1.1 copy-start.12
  18.4 8.6 %copy-start.19 = (s32[384,2]{0,1:T(2,128)S(1)}, s32[384,2]{0,1:T(2,128)}, u32[]{:S(2)}) copy-start(s32[384,2]{0,1:T(2,128)} %param.33) | copy-start | bytes 9220
  23.7 0.7 copy-start.4
  24.4 0.9 copy-start.15
  25.3 0.7 copy-start.17
  26.0 3.0 %copy-start.22 = (f32[384,2]{0,1:T(2,128)S(1)}, f32[384,2]{0,1:T(2,128)}, u32[]{:S(2)}) copy-start(f32[384,2]{0,1:T(2,128)} %param.34) | copy-start | bytes 9220
  26.1 4.3 %copy-start.8 = (f32[384,4,4]{0,2,1:T(4,128)}, f32[384,4,4]{0,2,1:T(4,128)S(1)}, u32[]{:S(2)}) copy-start(f32[384,4,4]{0,2,1:T(4,128)S(1)} %reshape.66) | copy-start | bytes 73732
  30.8 1.0 copy-start.5
  31.8 0.7 copy-start.9
  32.5 0.7 copy-start.10
  33.3 1.2 copy-start.16
  34.4 1.0 copy-start.18
  35.4 21.0 %copy-start.11 = (f32[1024]{0:T(1024)S(1)}, f32[1024]{0:T(1024)}, u32[]{:S(2)}) copy-start(f32[1024]{0:T(1024)} %param.30) | copy-start | bytes 12292
  39.2 1.1 copy-start.1
  56.4 1.4 copy-start.2
  57.8 1.1 copy-start.3
  59.0 1.0 copy-start.6
  60.0 6.2 %copy-start.7 = (bf16[384,512]{1,0:T(8,128)(2,1)S(1)}, bf16[384,512]{1,0:T(8,128)(2,1)}, u32[]{:S(2)}) copy-start(bf16[384,512]{1,0:T(8,128)(2,1)} %constant_dynamic-slice_fusion.stream_ref) | copy-start | bytes 1179652
  93.9 1.1 copy-start.14
  95.0 115.9 %copy-start.23 = (f32[384]{0:T(512)S(1)}, f32[384]{0:T(512)}, u32[]{:S(2)}) copy-start(f32[384]{0:T(512)} %get-tuple-element.17) | copy-start | bytes 4612
  95.0 115.9 %copy-start.24 = (f32[384]{0:T(512)S(1)}, f32[384]{0:T(512)}, u32[]{:S(2)}) copy-start(f32[384]{0:T(512)} %get-tuple-element.18) | copy-start | bytes 4612
  210.9 2.5 %copy-start.25 = (bf16[8,4,48,512]{3,2,1,0:T(8,128)(2,1)S(1)}, bf16[8,4,48,512]{3,2,1,0:T(8,128)(2,1)}, u32[]{:S(2)}) copy-start(bf16[8,4,48,512]{3,2,1,0:T(8,128)(2,1)} %shard_map.185) | copy-start | bytes 4718596
Sparse Core Ops, SparseCore 0:
  26.2 30.1 all-gather.2

commit v2 on v1

--- a/solution.py
+++ b/solution.py
@@ -329,6 +329,9 @@
         part = buf.at[dp, s, pl.ds(half, experts - half)]
         remote(part, part, far[0].at[k], far[1].at[k], (me, xp)).wait_recv()
 
+    ahead = list(range(planes))
+    later = ahead[1:] + ahead[:1]
+
     row_near = (x_send, x_recv, y_send, y_recv)
     row_far = (dx_send, dx_recv, dy_send, dy_recv)
     hid_near = (hx_send, hx_recv, hy_send, hy_recv)
@@ -355,7 +358,7 @@
             relay(rows_ref, j, c, row_near, row_far)
 
     def stage_c(j):
-        if j == 0:
+        if j == later[0]:
             loads[0].wait()
             loads[1].wait()
         for c in range(2):
@@ -385,7 +388,7 @@
     keep = []
 
     def stage_e(j):
-        if j == 0:
+        if j == later[0]:
             loads[2].wait()
         for c in range(2):
             arrive(hid_ref, j, c, hid_far)
@@ -416,12 +419,15 @@
                 )
             )
 
-    stages = (stage_a, stage_b, stage_c, stage_d, stage_e)
-    lag = (0, 1, 2, 3, 4)
-    for turn in range(planes + lag[-1]):
-        for stage, late in zip(stages, lag):
-            if 0 <= turn - late < planes:
-                stage(turn - late)
+    late = 2 if planes > 1 else 1
+    plan = (
+        (stage_a, ahead, 0), (stage_b, ahead, 1), (stage_c, later, late + 1),
+        (stage_d, later, late + 2), (stage_e, later, late + 3),
+    )
+    for turn in range(planes + late + 3):
+        for stage, order, lag in plan:
+            if 0 <= turn - lag < planes:
+                stage(order[turn - lag])
 
     keep[0].wait()
     for j in range(planes):

time: 223 us -> 217 us (0.973)
  Pallas kernels: 159 us -> 152 us
    pallas_call x1, Pallas kernels: 116 us -> 110 us  [run_experts(): pl.pallas_call(functools.partial(experts_kernel, n_sp, n_tp), out_shape=j...]
where the time goes in v2:
time: 217 us; the launch traced here: 216 us
  Pallas kernels  152 us (70%)
  local copies, waits for them, and re-layouts  21.7 us (10%)
  waiting for transfers between devices  16.1 us (7%)
  between operations  13.7 us (6%)
  matrix products  6.06 us (3%)
  starting transfers between devices  3.8 us (2%)
    pallas_call x1, Pallas kernels, run_experts(): pl.pallas_call(functools.partial(experts_kernel, n_sp, n_tp), out_shape=j...  110 us
    pallas_call x1, Pallas kernels, run_project(): pl.pallas_call(project_kernel, out_shape=(jax.ShapeDtypeStruct((length, s...  27.6 us
    all_gather x1, waiting for transfers between devices, per_device(): states = lax.all_gather(state, 'sp')  16.1 us
    unnamed x55, local copies, waits for them, and re-layouts  15.6 us
    pallas_call x1, Pallas kernels, per_device(): pl.pallas_call(functools.partial(outside_kernel, per_group), grid=(groups...  6.22 us
    pallas_call x1, Pallas kernels, per_device(): pl.pallas_call(functools.partial(conv_kernel, per_group), grid=(groups,),...  5.28 us
  transfers between devices with their start and end apart: 2, of which 1 were waited for; matrix products, arithmetic and copies ran while one was open for 4% of the time, Pallas kernels for 2%

profile of v2, /device:TPU:9, one launch (start us, length us, event | category | flops | bytes accessed | tf_op | source)
XLA Modules:
  0.0 215.6 jit_solution(16803140970350681306)
XLA Ops:
  6.6 0.8 slice_bitcast_fusion
  7.4 0.7 slice_bitcast_fusion.1
  8.1 0.7 slice.41
  8.8 3.8 %collective-permute-start = (bf16[8,2048]{1,0:T(8,128)(2,1)S(1)}, bf16[8,2048]{1,0:T(8,128)(2,1)S(1)}, u32[]{:S(2)}, u32[]{:S(2)}) collective-permute-start(bf16[8,2048]{1,0:T(8,128)(2,1)S(1)} %pad_maximum_fusion), channel_id=1, source_target_pairs={{0,4},{4,8},{8,12},{12,16},{16,20},{20,24},{24,28},{1,5},{5,9},{9,... | collective-permute-start | bytes 98312 | tf_op jit(solution)/shard_map/ppermute | solution.py:509
  12.6 0.7 exponential_negate_fusion
  13.3 1.3 fusion.23
  14.7 0.8 compare_select_fusion
  15.5 1.2 copy_bitcast_fusion
  17.3 1.1 copy-done.12
  18.4 5.3 %shard_map.181 = (bf16[384,1024]{1,0:T(8,128)(2,1)S(1)}, bf16[384,512]{1,0:T(8,128)(2,1)S(1)}, bf16[384,512]{1,0:T(8,128)(2,1)S(1)}, bf16[4,272,128]{2,1,0:T(8,128)(2,1)}) custom-call(bf16[384,1024]{1,0:T(8,128)(2,1)S(1)} %copy-done.12, bf16[384,512]{1,0:T(8,128)(2,1)S(1)} %get-tuple-element.28.w_ref, bf16[384,512]{1,0:T(8,128)(2,1)S(1)} %get-tuple-element.27.r_ref, ...), custom_call_target="tpu_custom_call" | custom-call | flops 1000000000 | bytes 10000000 | tf_op jit(solution)/shard_map/pallas_call | solution.py:529
  23.7 0.7 copy-done.4
  24.4 0.9 copy-done.15
  25.3 0.7 copy-done.17
  28.2 0.8 dynamic_slice.7
  29.6 0.8 constant_dynamic-slice_fusion.stream_ref
  30.8 1.0 copy-done.5
  31.8 0.7 copy-done.9
  32.5 0.7 copy-done.10
  33.3 1.2 copy-done.16
  34.4 1.0 copy-done.18
  35.4 3.8 %shard_map.182.in_ref = f32[384,1024]{1,0:T(8,128)S(1)} custom-call(bf16[384,1024]{1,0:T(8,128)(2,1)S(1)} %copy-done.16, bf16[384,512]{1,0:T(8,128)(2,1)S(1)} %copy-done.18, bf16[384,512]{1,0:T(8,128)(2,1)S(1)} %copy-done.5, f32[4,384,4]{2,1,0:T(8,128)S(1)} %bitcast.38, f32[4,4,384]{2,1,0:T(4,128)S(1)} %bitcast.41, f32[4,4,384]{2,1,0:T(4,128)S(1)} %bitcast.42), custom_call_target="tpu_custom_call" | custom-call | flops 4000000000 | bytes 10000000 | tf_op jit(solution)/shard_map/pallas_call | solution.py:559
  39.2 1.1 copy-done.1
  40.3 16.1 %all-gather.3.cloned.1.call-done = bf16[32,272,128]{2,1,0:T(8,128)(2,1)} async-done(((bf16[4,272,128]{2,1,0:T(8,128)(2,1)}), bf16[32,272,128]{2,1,0:T(8,128)(2,1)}) %all-gather.3.cloned.1.call-update) | async-done | bytes 2228240 | tf_op jit(solution)/shard_map/all_gather | solution.py:557
  56.4 1.4 copy-done.2
  57.8 1.1 copy-done.3
  59.0 1.0 copy-done.6
  60.0 6.2 %shard_map.183.mixed_ref = bf16[384,1024]{1,0:T(8,128)(2,1)S(1)} custom-call(f32[384,1024]{1,0:T(8,128)S(1)} %copy-done.2, bf16[384,512]{1,0:T(8,128)(2,1)S(1)} %copy-done.6, bf16[8,4,272,128]{3,2,1,0:T(8,128)(2,1)} %bitcast.47, f32[4,384,4]{2,1,0:T(8,128)S(1)} %bitcast.39, bf16[384,1024]{1,0:T(8,128)(2,1)S(1)} %copy-done.3, f32[1,1024]{1,0:T(1,128)S(1)} %bitcast.43), custom_call_target="tpu_custom_call" | custom-call | flops 1000000000 | bytes 10000000 | tf_op jit(solution)/shard_map/pallas_call | solution.py:574
  66.2 27.6 %shard_map.184 = (f32[384,512]{1,0:T(8,128)S(1)}, bf16[8,192,512]{2,1,0:T(8,128)(2,1)S(1)}) custom-call(bf16[384,1024]{1,0:T(8,128)(2,1)S(1)} %shard_map.183.mixed_ref, bf16[1024,2048]{1,0:T(8,128)(2,1)} %weight_ref.1, bf16[384,512]{1,0:T(8,128)(2,1)S(1)} %copy-done.7, f32[1,512]{1,0:T(1,128)S(1)} %bitcast.45, bf16[8,192,384]{2,1,0:T(8,128)(2,1)S(1)} %or_convert_fusion.place_ref), custom_call_target="tpu_custom_call" | custom-call | flops 4000000000 | bytes 10000000 | tf_op jit(solution)/shard_map/pallas_call | solution.py:214
  93.9 1.1 copy-done.14
  95.0 109.6 %shard_map.185 = bf16[8,4,48,512]{3,2,1,0:T(8,128)(2,1)} custom-call(bf16[8,4,48,512]{3,2,1,0:T(8,128)(2,1)} %bitcast.46, bf16[4,2048,256]{2,1,0:T(8,128)(2,1)} %gate_hbm.1, bf16[4,2048,256]{2,1,0:T(8,128)(2,1)} %up_hbm.1, bf16[4,1024,512]{2,1,0:T(8,128)(2,1)} %down_hbm.1), custom_call_target="tpu_custom_call" | custom-call | flops 10000000000 | bytes 20000000 | tf_op jit(solution)/shard_map/pallas_call | solution.py:466
  204.6 2.4 %fusion.19 = f32[384,512]{1,0:T(8,128)S(1)} fusion(bf16[1536,512]{1,0:T(8,128)(2,1)} %bitcast.52, f32[384]{0:T(512)S(1)} %copy-done.24, s32[384]{0:T(512)S(1)} %get-tuple-element.20, f32[384]{0:T(512)S(1)} %copy-done.23, s32[384]{0:T(512)S(1)} %get-tuple-element.19), kind=kOutput, calls=%fused_computation.20 | convolution fusion | flops 607518720 | bytes 2365440 | tf_op jit(solution)/shard_map/dot_general | solution.py:618
  207.0 1.8 fusion.3
  (65 shorter events, 3.8 us)
Async XLA Ops:
  6.5 23.1 %copy-start = (bf16[384,2048]{1,0:T(8,128)(2,1)S(1)}, bf16[384,2048]{1,0:T(8,128)(2,1)}, u32[]{:S(2)}) copy-start(bf16[384,2048]{1,0:T(8,128)(2,1)} %param.19) | copy-start | bytes 4718596
  6.5 10.2 %copy-start.21 = (bf16[4,4,128]{2,1,0:T(4,128)(2,1)S(1)}, bf16[4,4,128]{2,1,0:T(4,128)(2,1)}, u32[]{:S(2)}) copy-start(bf16[4,4,128]{2,1,0:T(4,128)(2,1)} %param.26) | copy-start | bytes 12292
  6.5 10.2 %copy-start.20 = (bf16[4,4,128]{2,1,0:T(4,128)(2,1)S(1)}, bf16[4,4,128]{2,1,0:T(4,128)(2,1)}, u32[]{:S(2)}) copy-start(bf16[4,4,128]{2,1,0:T(4,128)(2,1)} %param.27) | copy-start | bytes 12292
  6.5 10.7 %copy-start.13 = (bf16[4,1024]{1,0:T(4,128)(2,1)S(1)}, bf16[4,1024]{1,0:T(4,128)(2,1)}, u32[]{:S(2)}) copy-start(bf16[4,1024]{1,0:T(4,128)(2,1)} %kx_ref.1) | copy-start | bytes 24580
  6.5 49.9 %all-gather.3.cloned.1.call-start = ((), (), s32[]{:S(2)}) async-start(), calls=%async_computation | async-start | bytes 2506752 | tf_op jit(solution)/shard_map/all_gather | solution.py:557
  8.8 8.4 %collective-permute-start = (bf16[8,2048]{1,0:T(8,128)(2,1)S(1)}, bf16[8,2048]{1,0:T(8,128)(2,1)S(1)}, u32[]{:S(2)}, u32[]{:S(2)}) collective-permute-start(bf16[8,2048]{1,0:T(8,128)(2,1)S(1)} %pad_maximum_fusion), channel_id=1, source_target_pairs={{0,4},{4,8},{8,12},{12,16},{16,20},{20,24},{24,28},{1,5},{5,9},{9,... | collective-permute-start | bytes 98312 | tf_op jit(solution)/shard_map/ppermute | solution.py:509
  17.2 1.1 copy-start.12
  18.4 8.6 %copy-start.19 = (s32[384,2]{0,1:T(2,128)S(1)}, s32[384,2]{0,1:T(2,128)}, u32[]{:S(2)}) copy-start(s32[384,2]{0,1:T(2,128)} %param.33) | copy-start | bytes 9220
  23.7 0.7 copy-start.4
  24.4 0.9 copy-start.15
  25.3 0.7 copy-start.17
  26.0 3.0 %copy-start.22 = (f32[384,2]{0,1:T(2,128)S(1)}, f32[384,2]{0,1:T(2,128)}, u32[]{:S(2)}) copy-start(f32[384,2]{0,1:T(2,128)} %param.34) | copy-start | bytes 9220
  26.1 4.3 %copy-start.8 = (f32[384,4,4]{0,2,1:T(4,128)}, f32[384,4,4]{0,2,1:T(4,128)S(1)}, u32[]{:S(2)}) copy-start(f32[384,4,4]{0,2,1:T(4,128)S(1)} %reshape.66) | copy-start | bytes 73732
  30.8 1.0 copy-start.5
  31.8 0.7 copy-start.9
  32.5 0.7 copy-start.10
  33.3 1.2 copy-start.16
  34.4 1.0 copy-start.18
  35.4 21.0 %copy-start.11 = (f32[1024]{0:T(1024)S(1)}, f32[1024]{0:T(1024)}, u32[]{:S(2)}) copy-start(f32[1024]{0:T(1024)} %param.30) | copy-start | bytes 12292
  39.2 1.1 copy-start.1
  56.4 1.4 copy-start.2
  57.8 1.1 copy-start.3
  59.0 1.0 copy-start.6
  60.0 6.2 %copy-start.7 = (bf16[384,512]{1,0:T(8,128)(2,1)S(1)}, bf16[384,512]{1,0:T(8,128)(2,1)}, u32[]{:S(2)}) copy-start(bf16[384,512]{1,0:T(8,128)(2,1)} %constant_dynamic-slice_fusion.stream_ref) | copy-start | bytes 1179652
  93.9 1.1 copy-start.14
  95.0 109.6 %copy-start.23 = (f32[384]{0:T(512)S(1)}, f32[384]{0:T(512)}, u32[]{:S(2)}) copy-start(f32[384]{0:T(512)} %get-tuple-element.17) | copy-start | bytes 4612
  95.0 109.6 %copy-start.24 = (f32[384]{0:T(512)S(1)}, f32[384]{0:T(512)}, u32[]{:S(2)}) copy-start(f32[384]{0:T(512)} %get-tuple-element.18) | copy-start | bytes 4612
  204.6 2.5 %copy-start.25 = (bf16[8,4,48,512]{3,2,1,0:T(8,128)(2,1)S(1)}, bf16[8,4,48,512]{3,2,1,0:T(8,128)(2,1)}, u32[]{:S(2)}) copy-start(bf16[8,4,48,512]{3,2,1,0:T(8,128)(2,1)} %shard_map.185) | copy-start | bytes 4718596
Sparse Core Ops, SparseCore 0:
  26.2 30.1 all-gather.2
